TPU v7x, 32 devices: a whole 2x2x4 slice. The times are simulated.
32 devices in a mesh: sp: 4 (over y, x), tp: 8 (over z, core).
Axes of the slice: x: 2, y: 2, z: 4, core: 2. Of those that a mesh axis runs over, the one named last changes fastest.
Arguments:
- query_vectors: bfloat16 [4096, 16, 128], P('sp', 'tp'), may hold values from -6 to 6
- key_vectors: bfloat16 [4096, 16, 128], P('sp', 'tp'), may hold values from -6 to 6
- value_vectors: bfloat16 [4096, 16, 128], P('sp', 'tp'), may hold values from -6 to 6
- out_gate: bfloat16 [4096, 16, 128], P('sp', 'tp'), may hold values from -6 to 6
- decay_rate: float32 [2, 16], P(None, 'tp'), may hold values from 0 to 1
- decay_pre: float32 [2, 16, 4096], P(None, 'tp', 'sp'), may hold values from -6 to 6
- decay_shock: float32 [2, 16, 4096], P(None, 'tp', 'sp'), may hold values from -2 to 0
- beta_pre: float32 [2, 16, 4096], P(None, 'tp', 'sp'), may hold values from -12 to 0
- head_gain: float32 [128], replicated, may hold values from 0.1 to 1.9
- w_out: bfloat16 [2048, 2048], P('tp'), may hold values from -0.125 to 0.125
- tokens: bfloat16 [4096, 2048], P(('sp', 'tp')), may hold values from -6 to 6
- norm_gain: float32 [2048], replicated, may hold values from 0.1 to 1.9
- experts_pick: int32 [4096, 2], P(('sp', 'tp')), may hold values from 0 to 3, as said below
- pair_logits: float32 [4096, 2], P(('sp', 'tp')), may hold values from -6 to 6
- group_logits: float32 [4096, 2], P(('sp', 'tp')), may hold values from -6 to 6
- expert_gate: bfloat16 [4, 2048, 2048], P('sp', None, 'tp'), may hold values from -0.125 to 0.125
- expert_up: bfloat16 [4, 2048, 2048], P('sp', None, 'tp'), may hold values from -0.125 to 0.125
- expert_down: bfloat16 [4, 2048, 2048], P('sp', None, 'tp'), may hold values from -0.5 to 0.5
Outputs:
- layer_out: bfloat16 [4096, 2048], P(('sp', 'tp'))
Inputs may be any that keep to these rules, and one draw needn't show every extreme that they name: `experts_pick`: each token names two different experts of one group of 2 consecutive experts. The 128 tokens of one device fall 64 into each group. At most 64 tokens of one device name any one expert, and in every draw every expert is named by 64 tokens of every device.
All inputs are finite; a program needn't handle non-finite values.
Results may differ from a plain program's by a relative error of at most 0.02.
Values may be sent and summed in bfloat16 or wider, within the bound.
A program may use at most 128 MiB of HBM per device.

v0:
```python
import jax
import jax.numpy as jnp
from jax import lax
from jax.sharding import PartitionSpec as P

BLOCK = 64
GROUP_SIZE = 2


NORM_EPSILON = 1e-06
EXACT_PRECISION = lax.Precision.HIGHEST


def unit_rows(vectors):
    return vectors * lax.rsqrt(jnp.sum(vectors * vectors, axis=-1, keepdims=True) + NORM_EPSILON)


def block_sweep(queries, key_rows, value_rows, log_decay, beta_rate, start_state):
    length, value_width = value_rows.shape
    blocks = length // BLOCK
    query_blocks = queries.reshape(blocks, BLOCK, queries.shape[1])
    key_blocks = key_rows.reshape(blocks, BLOCK, key_rows.shape[1])
    value_blocks = value_rows.reshape(blocks, BLOCK, value_width)
    cumulative = jnp.cumsum(log_decay.reshape(blocks, BLOCK), axis=1)
    beta_blocks = beta_rate.reshape(blocks, BLOCK)
    position = jnp.arange(BLOCK)
    lower_mask = position[:, None] >= position[None, :]
    strict = position[:, None] > position[None, :]
    spread = cumulative[:, :, None] - cumulative[:, None, :]
    within = jnp.where(lower_mask, jnp.exp(jnp.where(lower_mask, spread, 0.0)), 0.0)
    scaled_keys = key_blocks * beta_blocks[:, :, None]
    lower_matrix = jnp.where(
        strict,
        jnp.einsum("nid,njd->nij", scaled_keys, key_blocks, precision=EXACT_PRECISION) * within,
        0.0,
    )
    identity = jnp.eye(BLOCK, dtype=jnp.float32)
    right_side = jnp.concatenate(
        [value_blocks * beta_blocks[:, :, None], scaled_keys * jnp.exp(cumulative)[:, :, None]],
        axis=2,
    )
    solved = jax.scipy.linalg.solve_triangular(
        lower_matrix + identity, right_side, lower=True, unit_diagonal=True
    )
    fresh_values = solved[:, :, :value_width]
    corrections = solved[:, :, value_width:]
    scores = (
        jnp.einsum("nid,njd->nij", query_blocks, key_blocks, precision=EXACT_PRECISION) * within
    )
    query_decayed = query_blocks * jnp.exp(cumulative)[:, :, None]
    block_total = cumulative[:, -1]
    decayed_keys = key_blocks * jnp.exp(block_total[:, None] - cumulative)[:, :, None]

    def advance(carried, inputs):
        values_in, fix_rows, query_in, key_in, score_in, total_in = inputs
        updated = values_in - jnp.dot(fix_rows, carried, precision=EXACT_PRECISION)
        output = jnp.dot(query_in, carried, precision=EXACT_PRECISION) + jnp.dot(
            score_in, updated, precision=EXACT_PRECISION
        )
        carried = carried * jnp.exp(total_in) + jnp.dot(
            key_in.T, updated, precision=EXACT_PRECISION
        )
        return (carried, output)

    final_state, outputs = lax.scan(
        advance,
        start_state,
        (fresh_values, corrections, query_decayed, decayed_keys, scores, block_total),
    )
    return (outputs.reshape(length, value_width), final_state)


def shards(
    query_vectors,
    key_vectors,
    value_vectors,
    out_gate,
    decay_rate,
    decay_pre,
    decay_shock,
    beta_pre,
    head_gain,
    w_out,
    tokens,
    norm_gain,
    experts_pick,
    pair_logits,
    group_logits,
    expert_gate,
    expert_up,
    expert_down,
):
    per_head_width = query_vectors.shape[2]
    queries = unit_rows(
        jnp.transpose(query_vectors.astype(jnp.float32), (1, 0, 2))
    ) * per_head_width ** (-0.5)
    keyset = unit_rows(jnp.transpose(key_vectors.astype(jnp.float32), (1, 0, 2)))
    valueset = jnp.transpose(value_vectors.astype(jnp.float32), (1, 0, 2))
    padded_values = jnp.concatenate([valueset, jnp.zeros_like(keyset)], axis=2)
    log_decay = jnp.moveaxis(
        -decay_rate[:, :, None] * jax.nn.softplus(decay_pre) + decay_shock, 1, 0
    )
    beta_rate = jnp.moveaxis(jax.nn.sigmoid(beta_pre), 1, 0)
    identity = jnp.eye(per_head_width, dtype=jnp.float32)
    opening = jnp.concatenate(
        [jnp.zeros((per_head_width, per_head_width), jnp.float32), identity], axis=1
    )

    def one_head(query_head, key_head, value_head, decay_head, beta_head):
        forward_result, ahead_end = block_sweep(
            query_head, key_head, value_head, decay_head[0], beta_head[0], opening
        )
        trailing_part, behind_end = block_sweep(
            query_head[::-1],
            key_head[::-1],
            value_head[::-1],
            decay_head[1, ::-1],
            beta_head[1, ::-1],
            opening,
        )
        return (forward_result, trailing_part[::-1], ahead_end, behind_end)

    forward_result, trailing_part, ahead_end, behind_end = jax.vmap(one_head)(
        queries, keyset, padded_values, log_decay, beta_rate
    )
    forward_shift = ahead_end[:, :, per_head_width:]
    forward_add = ahead_end[:, :, :per_head_width]
    backward_shift = behind_end[:, :, per_head_width:]
    backward_add = behind_end[:, :, :per_head_width]
    collected = (
        lax.all_gather(forward_shift[None].astype(jnp.bfloat16), "sp", axis=0, tiled=True).astype(
            jnp.float32
        ),
        lax.all_gather(forward_add[None].astype(jnp.bfloat16), "sp", axis=0, tiled=True).astype(
            jnp.float32
        ),
        lax.all_gather(backward_shift[None].astype(jnp.bfloat16), "sp", axis=0, tiled=True).astype(
            jnp.float32
        ),
        lax.all_gather(backward_add[None].astype(jnp.bfloat16), "sp", axis=0, tiled=True).astype(
            jnp.float32
        ),
    )
    own_index = lax.axis_index("sp")
    device_total = lax.axis_size("sp")

    def fold_forward(device_index, carried):
        applied = (
            jnp.einsum(
                "hij,hjv->hiv", collected[0][device_index], carried, precision=EXACT_PRECISION
            )
            + collected[1][device_index]
        )
        return jnp.where(device_index < own_index, applied, carried)

    def fold_backward(device_index, carried):
        mirrored = device_total - 1 - device_index
        applied = (
            jnp.einsum("hij,hjv->hiv", collected[2][mirrored], carried, precision=EXACT_PRECISION)
            + collected[3][mirrored]
        )
        return jnp.where(mirrored > own_index, applied, carried)

    zero_state = jnp.zeros_like(forward_add)
    forward_carried = lax.fori_loop(0, device_total, fold_forward, zero_state)
    backward_carried = lax.fori_loop(0, device_total, fold_backward, zero_state)
    joined = (
        forward_result[:, :, :per_head_width]
        + trailing_part[:, :, :per_head_width]
        + jnp.einsum(
            "qfc,qcj->qfj",
            forward_result[:, :, per_head_width:],
            forward_carried,
            precision=EXACT_PRECISION,
        )
        + jnp.einsum(
            "qfc,qcj->qfj",
            trailing_part[:, :, per_head_width:],
            backward_carried,
            precision=EXACT_PRECISION,
        )
    )
    joined = jnp.transpose(joined, (1, 0, 2))
    head_scale = lax.rsqrt(jnp.mean(joined * joined, axis=-1, keepdims=True) + NORM_EPSILON)
    mixed_heads = (
        joined * head_scale * head_gain * jax.nn.silu(out_gate.astype(jnp.float32))
    ).astype(jnp.bfloat16)
    mixed_heads = mixed_heads.reshape(joined.shape[0], joined.shape[1] * per_head_width)
    local_rows = tokens.shape[0]
    part_sum = jnp.dot(mixed_heads, w_out, preferred_element_type=jnp.float32).astype(jnp.bfloat16)
    branch_sum = lax.psum_scatter(
        lax.optimization_barrier(part_sum).astype(jnp.float32).astype(jnp.bfloat16),
        "tp",
        scatter_dimension=0,
        tiled=True,
    ).astype(jnp.float32)
    residual = tokens.astype(jnp.float32) + branch_sum
    normed = (
        residual
        * lax.rsqrt(jnp.mean(residual * residual, axis=-1, keepdims=True) + NORM_EPSILON)
        * norm_gain
    ).astype(jnp.bfloat16)
    group_count = group_logits.shape[1]
    group_exp = jnp.exp(group_logits)
    group_share = group_exp / jnp.sum(group_exp, axis=-1, keepdims=True)
    group_index_of = experts_pick[:, 0] // GROUP_SIZE
    group_weight = jnp.sum(
        jnp.where(jnp.arange(group_count)[None, :] == group_index_of[:, None], group_share, 0.0),
        axis=1,
    )
    pair_exp = jnp.exp(pair_logits)
    route_weight = pair_exp / jnp.sum(pair_exp, axis=-1, keepdims=True) * group_weight[:, None]
    capacity = local_rows // group_count
    expert_count = lax.axis_size("sp")
    expert_marks = jnp.sum(
        (
            experts_pick[:, :, None] == jnp.arange(expert_count, dtype=jnp.int32)[None, None, :]
        ).astype(jnp.int32),
        axis=1,
    )
    earlier = jnp.cumsum(expert_marks, axis=0) - expert_marks
    slot_place = experts_pick * capacity + jnp.take_along_axis(earlier, experts_pick, axis=1)
    slot_index = jnp.arange(expert_count * capacity, dtype=jnp.int32)[:, None]
    chooser = (
        (slot_index == slot_place[None, :, 0]) | (slot_index == slot_place[None, :, 1])
    ).astype(jnp.bfloat16)
    outgoing = jnp.dot(chooser, normed, preferred_element_type=jnp.float32).astype(jnp.bfloat16)
    outgoing = outgoing.reshape(expert_count, capacity, normed.shape[1])
    arrived = lax.all_to_all(outgoing, "sp", split_axis=0, concat_axis=0, tiled=True)
    source_count, slot_count, model_width = arrived.shape
    row_count = source_count * slot_count
    flat_rows = arrived.reshape(row_count, model_width)
    part_rows = lax.all_gather(flat_rows, "tp", axis=0, tiled=True)
    gate_out = jnp.dot(part_rows, expert_gate[0], preferred_element_type=jnp.float32)
    up_out = jnp.dot(part_rows, expert_up[0], preferred_element_type=jnp.float32)
    hidden = (jax.nn.silu(gate_out) * up_out).astype(jnp.bfloat16)
    product = lax.dot_general(
        hidden, expert_down[0], (((1,), (1,)), ((), ())), preferred_element_type=jnp.float32
    ).astype(jnp.bfloat16)
    summed_out = lax.psum_scatter(
        lax.optimization_barrier(product).astype(jnp.float32).astype(jnp.bfloat16),
        "tp",
        scatter_dimension=0,
        tiled=True,
    )
    expert_rows = summed_out.reshape(source_count, slot_count, model_width)
    results = lax.all_to_all(expert_rows, "sp", split_axis=0, concat_axis=0, tiled=True)
    gathered = results.reshape(expert_count * capacity, normed.shape[1])
    chosen = gathered[slot_place]
    mixture = jnp.einsum("tk,tkd->td", route_weight, chosen.astype(jnp.float32))
    return (residual + mixture).astype(jnp.bfloat16)


def solution(mesh):
    return jax.shard_map(
        shards,
        mesh=mesh,
        in_specs=(
            P("sp", "tp", None),
            P("sp", "tp", None),
            P("sp", "tp", None),
            P("sp", "tp", None),
            P(None, "tp"),
            P(None, "tp", "sp"),
            P(None, "tp", "sp"),
            P(None, "tp", "sp"),
            P(),
            P("tp", None),
            P(("sp", "tp"), None),
            P(),
            P(("sp", "tp"), None),
            P(("sp", "tp"), None),
            P(("sp", "tp"), None),
            P("sp", None, "tp"),
            P("sp", None, "tp"),
            P("sp", None, "tp"),
        ),
        out_specs=P(("sp", "tp"), None),
        check_vma=False,
    )
```

profile of v0, /device:TPU:0, one launch (start us, length us, event | category | flops | bytes accessed | tf_op | source)
XLA Modules:
  0.0 939.8 jit_solution(3819196034721177921)
XLA Ops:
  20.8 5.0 reverse.5
  30.2 158.0 %custom-call.9 = f32[2,16,1,64,64]{3,4,2,1,0:T(8,128)} custom-call(f32[2,16,1,64,64]{4,3,2,1,0:T(8,128)S(1)} %fusion.84), custom_call_target="InvertDiagBlocksLowerTriangular" | custom-call | tf_op jit(solution)/shard_map/vmap(jit(_solve_triangular))/vmap()/triangular_solve | solution.py:42
  208.2 3.6 fusion.99
  211.8 158.0 %custom-call.8 = f32[2,16,1,64,64]{3,4,2,1,0:T(8,128)} custom-call(f32[2,16,1,64,64]{4,3,2,1,0:T(8,128)S(1)} %fusion.99), custom_call_target="InvertDiagBlocksLowerTriangular" | custom-call | tf_op jit(solution)/shard_map/vmap(jit(_solve_triangular))/vmap()/triangular_solve | solution.py:42
  381.1 4.4 fusion.70
  388.7 97.6 %while.55 = (s32[]{:T(128)}, f32[2,128,256]{2,1,0:T(8,128)S(1)}, f32[16,2,64,256]{3,2,1,0:T(8,128)}, f32[16,2]{1,0:T(8,128)}, f32[16,2,64,128]{3,2,0,1:T(8,128)}...) while((s32[]{:T(128)}, f32[2,128,256]{2,1,0:T(8,128)S(1)}, ...), condition=%wide.region_7.9_spmd, body=%wide.region_6.8_spmd.sunk | while | flops 176357376 | bytes 2231425 | solution.py:65
  486.3 10.6 %all-gather.2 = bf16[8,128,128]{2,1,0:T(8,128)(2,1)S(1)} all-gather(bf16[2,128,128]{2,1,0:T(8,128)(2,1)S(1)} %get-tuple-element.581), channel_id=4, replica_groups=mesh['sp'=4,'tp'=8] {'sp'}, dimensions={0}, use_global_device_ids=true | all-gather | bytes 327680 | tf_op jit(solution)/shard_map/all_gather | solution.py:137
  497.7 8.9 all-gather.3
  507.5 5.2 while.57
  512.7 3.5 fusion.71
  517.2 76.5 %while.54 = (s32[]{:T(128)}, f32[2,128,256]{2,1,0:T(8,128)S(1)}, f32[16,2,64,256]{3,2,1,0:T(8,128)S(1)}, f32[16,2]{1,0:T(8,128)S(1)}, f32[16,2,64,128]{3,2,0,1:T...) while((s32[]{:T(128)}, f32[2,128,256]{2,1,0:T(8,128)S(1)}, ...), condition=%wide.region_4.6_spmd, body=%wide.region_3.5_spmd.sunk | while | flops 176357376 | bytes 2231425 | solution.py:65
  593.8 8.1 all-gather
  602.7 8.9 all-gather.1
  612.5 5.3 while.56
  620.9 8.8 slice.89
  631.2 8.9 slice.94
  651.9 46.9 %reduce-scatter.3.cloned.1.call-done = bf16[128,2048]{1,0:T(8,128)(2,1)} async-done(((bf16[1024,2048]{1,0:T(8,128)(2,1)}), bf16[128,2048]{1,0:T(8,128)(2,1)}) %reduce-scatter.3.cloned.1.call-update) | async-done | bytes 524304 | tf_op jit(solution)/shard_map/reduce_scatter | solution.py:191
  701.7 16.0 %all_to_all.10 = bf16[4,64,2048]{2,1,0:T(8,128)(2,1)} all-to-all(bf16[4,64,2048]{2,1,0:T(8,128)(2,1)S(1)} %bitcast.279), channel_id=1, replica_groups=mesh['sp'=4,'tp'=8] {'sp'}, dimensions={0} | all-to-all | bytes 2097152 | tf_op jit(solution)/shard_map/all_to_all | solution.py:229
  717.7 81.0 %all-gather.6.cloned.1.call-done = bf16[2048,2048]{1,0:T(8,128)(2,1)} async-done(((bf16[256,2048]{1,0:T(8,128)(2,1)}), bf16[2048,2048]{1,0:T(8,128)(2,1)}) %all-gather.6.cloned.1.call-update) | async-done | bytes 8388624 | tf_op jit(solution)/shard_map/all_gather | solution.py:233
  798.7 7.1 fusion.111
  805.8 17.0 %convolution_convert_fusion = bf16[2048,2048]{1,0:T(8,128)(2,1)} fusion(bf16[2048,2048]{1,0:T(8,128)(2,1)} %all-gather.6.cloned.1.call-done, f32[2048,256]{1,0:T(8,128)} %fusion.111, bf16[1,2048,256]{2,1,0:T(8,128)(2,1)S(1)} %copy-done, bf16[1,2048,256]{2,1,0:T(8,128)(2,1)} %param.44), kind=kOutput, calls=%fused_computation.62 | convolution fusion | flops 4302307328 | bytes 20971520 | tf_op jit(solution)/shard_map/dot_general | solution.py:237
  822.8 88.1 %reduce-scatter.5.cloned.1.call-done = bf16[256,2048]{1,0:T(8,128)(2,1)} async-done(((bf16[2048,2048]{1,0:T(8,128)(2,1)}), bf16[256,2048]{1,0:T(8,128)(2,1)}) %reduce-scatter.5.cloned.1.call-update) | async-done | bytes 1048592 | tf_op jit(solution)/shard_map/reduce_scatter | solution.py:240
  910.9 3.6 all-to-all-start.1
  915.1 11.4 %all-to-all-done.1 = bf16[4,64,2048]{2,1,0:T(8,128)(2,1)S(1)} async-done(((bf16[4,64,2048]{2,1,0:T(8,128)(2,1)}), bf16[4,64,2048]{2,1,0:T(8,128)(2,1)S(1)}, u32[]{:S(2)}, u32[]{:S(2)}) %all-to-all-start.1) | async-done | bytes 1048608 | tf_op jit(solution)/shard_map/all_to_all | solution.py:247
  (340 shorter events, 266.2 us)
Async XLA Ops:
  6.5 799.2 %copy-start = (bf16[1,2048,256]{2,1,0:T(8,128)(2,1)S(1)}, bf16[1,2048,256]{2,1,0:T(8,128)(2,1)}, u32[]{:S(2)}) copy-start(bf16[1,2048,256]{2,1,0:T(8,128)(2,1)} %param.45) | copy-start | bytes 3145732
  6.5 5.5 copy-start.14
  6.5 692.2 %reduce-scatter.3.cloned.1.call-start = ((), (), s32[]{:S(2)}) async-start(), calls=%async_computation.4 | async-start | bytes 4718592 | tf_op jit(solution)/shard_map/reduce_scatter | solution.py:191
  16.2 12.0 %copy-start.3 = (f32[2,1024,128]{2,1,0:T(8,128)}, f32[2,1024,128]{2,1,0:T(8,128)S(1)}, u32[]{:S(2)}) copy-start(f32[2,1024,128]{2,1,0:T(8,128)S(1)} %copy.278) | copy-start | bytes 3145732
  28.2 352.9 %copy-start.20 = (pred[64,64]{1,0:T(8,128)(4,1)}, pred[64,64]{1,0:T(8,128)(4,1)S(1)}, u32[]{:S(2)}) copy-start(pred[64,64]{1,0:T(8,128)(4,1)S(1)} %get-tuple-element.599) | copy-start | bytes 12292
  195.3 2.2 copy-start.16
  208.0 163.8 %copy-start.22 = (f32[2,16]{1,0:T(2,128)}, f32[2,16]{1,0:T(2,128)S(1)}, u32[]{:S(2)}) copy-start(f32[2,16]{1,0:T(2,128)S(1)} %slice_reduce_fusion.1) | copy-start | bytes 388
  369.8 2.1 copy-start.1
  369.8 2.2 copy-start.2
  371.9 2.5 copy-start.17
  486.3 21.3 %copy-start.8 = (f32[2,128,128]{2,1,0:T(8,128)S(1)}, f32[2,128,128]{2,1,0:T(8,128)}, u32[]{:S(2)}) copy-start(f32[2,128,128]{2,1,0:T(8,128)} %custom-call.7) | copy-start | bytes 393220
  512.7 4.3 copy-start.9
  512.7 4.3 copy-start.15
  631.2 8.9 copy-start.7
  640.2 2.4 copy-start.10
  640.2 2.5 copy-start.13
  648.4 150.3 %all-gather.6.cloned.1.call-start = ((), (), s32[]{:S(2)}) async-start(), calls=%async_computation.5 | async-start | bytes 9437184 | tf_op jit(solution)/shard_map/all_gather | solution.py:233
  649.7 49.1 %copy-start.11 = (bf16[128,2048]{1,0:T(8,128)(2,1)S(1)}, bf16[128,2048]{1,0:T(8,128)(2,1)}, u32[]{:S(2)}) copy-start(bf16[128,2048]{1,0:T(8,128)(2,1)} %param.38) | copy-start | bytes 1572868
  649.7 50.4 %copy-start.24 = (f32[2048]{0:T(1024)S(1)}, f32[2048]{0:T(1024)}, u32[]{:S(2)}) copy-start(f32[2048]{0:T(1024)} %param.39) | copy-start | bytes 24580
  701.7 97.1 %copy-start.28 = (bf16[1,2048,256]{2,1,0:T(8,128)(2,1)S(1)}, bf16[1,2048,256]{2,1,0:T(8,128)(2,1)}, u32[]{:S(2)}) copy-start(bf16[1,2048,256]{2,1,0:T(8,128)(2,1)} %param.43) | copy-start | bytes 3145732
  717.7 193.3 %reduce-scatter.5.cloned.1.call-start = ((), (), s32[]{:S(2)}) async-start(), calls=%async_computation.6 | async-start | bytes 9437184 | tf_op jit(solution)/shard_map/reduce_scatter | solution.py:240
  822.8 92.1 %copy-start.26 = (f32[128,2]{0,1:T(2,128)S(1)}, f32[128,2]{0,1:T(2,128)}, u32[]{:S(2)}) copy-start(f32[128,2]{0,1:T(2,128)} %param.42) | copy-start | bytes 3076
  822.8 92.1 %copy-start.25 = (f32[128,2]{0,1:T(2,128)S(1)}, f32[128,2]{0,1:T(2,128)}, u32[]{:S(2)}) copy-start(f32[128,2]{0,1:T(2,128)} %param.41) | copy-start | bytes 3076
  910.9 15.5 %all-to-all-start.1 = ((bf16[4,64,2048]{2,1,0:T(8,128)(2,1)}), bf16[4,64,2048]{2,1,0:T(8,128)(2,1)S(1)}, u32[]{:S(2)}, u32[]{:S(2)}) async-start(bf16[4,64,2048]{2,1,0:T(8,128)(2,1)} %bitcast.285), calls=%async_computation.3 | async-start | bytes 2097152 | tf_op jit(solution)/shard_map/all_to_all | solution.py:247
  (9 other events, 10.4 us)
Sparse Core Ops, SparseCore 0:
  648.6 50.1 reduce-scatter.2
  717.8 80.8 all-gather.5
  822.9 88.0 reduce-scatter.4
where the time goes:
time: 954 us; the launch traced here: 940 us
  other arithmetic  346 us (36%)
  waiting for transfers between devices  227 us (24%)
  matrix products  225 us (24%)
  local copies, waits for them, and re-layouts  69.5 us (7%)
  blocking collectives  52.5 us (6%)
  between operations  13.9 us (1%)
    another operation x5, other arithmetic, block_sweep(): jax.scipy.linalg.solve_triangular(lower_matrix + identity, right_side, lo...  316 us
    reduce_scatter x1, waiting for transfers between devices, shards(): lax.psum_scatter(lax.optimization_barrier(product).astype(jnp.float32).as...  88.1 us
    all_gather x1, waiting for transfers between devices, shards(): part_rows = lax.all_gather(flat_rows, 'tp', axis=0, tiled=True)  81 us
    reduce_scatter x1, waiting for transfers between devices, shards(): lax.psum_scatter(lax.optimization_barrier(part_sum).astype(jnp.float32).a...  46.9 us
    dot_general x32, matrix products, advance(): jnp.dot(score_in, updated, precision=EXACT_PRECISION)  45.7 us
    dot_general x32, matrix products, advance(): jnp.dot(key_in.T, updated, precision=EXACT_PRECISION)  40.6 us
    dot_general x32, matrix products, advance(): updated = values_in - jnp.dot(fix_rows, carried, precision=EXACT_PRECISION)  39.1 us
    dot_general x32, matrix products, advance(): jnp.dot(query_in, carried, precision=EXACT_PRECISION)  35.8 us
  transfers between devices with their start and end apart: 4, of which 4 were waited for; matrix products, arithmetic and copies ran while one was open for 0% of the time, Pallas kernels for 0%

commit v1 on v0

v1 whole, which is shorter than its diff:
```python
import functools

import jax
import jax.numpy as jnp
from jax import lax
from jax.experimental import pallas as pl
from jax.experimental.pallas import tpu as pltpu
from jax.sharding import PartitionSpec as P

GROUP_SIZE = 2

NORM_EPSILON = 1e-06
EXACT_PRECISION = lax.Precision.HIGHEST
F32 = jnp.float32
BF16 = jnp.bfloat16
VMEM = pl.BlockSpec(memory_space=pltpu.VMEM)
SMEM = pl.BlockSpec(memory_space=pltpu.SMEM)


def mm(left, right, contract=((1,), (0,))):
    return lax.dot_general(left, right, (contract, ((), ())), preferred_element_type=F32)


def chunk_kernel(
    heads, q_ref, k_ref, v_ref, decay_ref, beta_ref,
    base_ref, lift_ref, ends_ref,
    stack_ref, add_ref, cum_ref, total_ref, state_ref,
):
    length = q_ref.shape[0]
    width = q_ref.shape[1] // heads
    size = decay_ref.shape[1]
    chunks = length // size
    half = heads * chunks
    row = lax.broadcasted_iota(jnp.int32, (size, size), 0)
    col = lax.broadcasted_iota(jnp.int32, (size, size), 1)
    exact = functools.partial(jnp.dot, precision=EXACT_PRECISION, preferred_element_type=F32)
    ones_up = jnp.where(row <= col, 1.0, 0.0).astype(F32)
    ones_down = jnp.where(row >= col, 1.0, 0.0).astype(F32)
    cum_ref[:half, :] = exact(decay_ref[:half, :], ones_up)
    cum_ref[half:, :] = exact(decay_ref[half:, :], ones_down)
    levels = size.bit_length() - 1

    def prepare(chunk, carry):
        start = pl.multiple_of(chunk * size, size)
        rows = pl.ds(start, size)
        distance = row ^ col
        eye = row == col
        units = []
        for head in range(heads):
            lanes = slice(head * width, (head + 1) * width)
            query = q_ref[rows, lanes].astype(F32)
            query = query * lax.rsqrt(jnp.sum(query * query, axis=1, keepdims=True) + NORM_EPSILON)
            query = query * width ** (-0.5)
            key = k_ref[rows, lanes].astype(F32)
            key = key * lax.rsqrt(jnp.sum(key * key, axis=1, keepdims=True) + NORM_EPSILON)
            value = v_ref[rows, lanes].astype(F32)
            key_low = key.astype(BF16)
            gram = mm(key_low, key_low, ((1,), (1,)))
            score = mm(query.astype(BF16), key_low, ((1,), (1,)))
            for way in range(2):
                unit = (way * heads + head) * chunks + chunk
                cum_row = cum_ref[pl.ds(unit, 1), :]
                beta_row = beta_ref[pl.ds(unit, 1), :]
                cum_col = jnp.sum(jnp.where(eye, cum_row, 0.0), axis=1, keepdims=True)
                beta_col = jnp.sum(jnp.where(eye, beta_row, 0.0), axis=1, keepdims=True)
                total = cum_row[:, size - 1 :] if way == 0 else cum_row[:, :1]
                seen = row >= col if way == 0 else row <= col
                within = jnp.where(seen, jnp.exp(jnp.where(seen, cum_col - cum_row, 0.0)), 0.0)
                lower = jnp.where(eye, 0.0, gram * within * beta_col)
                decayed = jnp.exp(cum_col)
                right = jnp.concatenate([key * (beta_col * decayed), value * beta_col], axis=1)
                total_ref[pl.ds(unit, 1), :] = jnp.broadcast_to(jnp.exp(total), (1, size))
                units.append(
                    dict(
                        unit=unit, head=head, way=way, lower=lower,
                        inverse=(jnp.where(eye, 1.0, 0.0) - jnp.where(distance == 1, lower, 0.0)).astype(BF16),
                        right=right.astype(BF16),
                        score=(score * within).astype(BF16),
                        query=query * decayed,
                        key=(key * jnp.exp(total - cum_col)).astype(BF16),
                    )
                )
        for level in range(1, levels):
            here = (distance >> level) == 1
            firsts = [
                mm(item["inverse"], jnp.where(here, item["lower"], 0.0).astype(BF16)).astype(BF16)
                for item in units
            ]
            seconds = [mm(first, item["inverse"]) for first, item in zip(firsts, units)]
            for item, second in zip(units, seconds):
                item["inverse"] = (item["inverse"].astype(F32) - second).astype(BF16)
        solved = [mm(item["inverse"], item["right"]).astype(BF16) for item in units]
        outs = [mm(item["score"], both) for item, both in zip(units, solved)]
        maps = [mm(item["key"], both, ((0,), (0,))) for item, both in zip(units, solved)]
        base = [None] * heads
        for item, out, change in zip(units, outs, maps):
            unit = item["unit"]
            stack_ref[unit, :size, :] = (item["query"] - out[:, :width]).astype(BF16)
            stack_ref[unit, size:, :] = change[:, :width].astype(BF16)
            add_ref[unit] = change[:, width:]
            fresh = out[:, width:]
            head = item["head"]
            base[head] = fresh if base[head] is None else base[head] + fresh
        for head in range(heads):
            base_ref[rows, head * width : (head + 1) * width] = base[head]
        return carry

    lax.fori_loop(0, chunks, prepare, 0)

    wide_row = lax.broadcasted_iota(jnp.int32, (width, 2 * width), 0)
    wide_col = lax.broadcasted_iota(jnp.int32, (width, 2 * width), 1)
    opening = jnp.where(wide_row + width == wide_col, 1.0, 0.0).astype(F32)
    for chain in range(2 * heads):
        state_ref[chain] = opening

    def advance(step, carry):
        for way in range(2):
            chunk = step if way == 0 else chunks - 1 - step
            rows = pl.ds(pl.multiple_of(chunk * size, size), size)
            for head in range(heads):
                chain = way * heads + head
                unit = chain * chunks + chunk
                state = state_ref[chain]
                both = mm(stack_ref[unit], state.astype(BF16))
                lanes = slice(head * width, (head + 1) * width)
                base_ref[rows, lanes] += both[:size, :width]
                lift_ref[chain, rows, :] = both[:size, width:].astype(BF16)
                keep = total_ref[pl.ds(unit, 1), :width]
                state_ref[chain, :, :width] = (
                    state[:, :width] * keep - both[size:, :width] + add_ref[unit]
                )
                state_ref[chain, :, width:] = state[:, width:] * keep - both[size:, width:]
        return carry

    lax.fori_loop(0, chunks, advance, 0)
    for chain in range(2 * heads):
        ends_ref[chain] = state_ref[chain].astype(BF16)


def chunk_maps(heads, queries, keys, values, decay, beta):
    length = queries.shape[0]
    width = queries.shape[1] // heads
    units, size = decay.shape
    return pl.pallas_call(
        functools.partial(chunk_kernel, heads),
        out_shape=(
            jax.ShapeDtypeStruct((length, heads * width), F32),
            jax.ShapeDtypeStruct((2 * heads, length, width), BF16),
            jax.ShapeDtypeStruct((2 * heads, width, 2 * width), BF16),
        ),
        in_specs=[VMEM] * 5,
        out_specs=(VMEM, VMEM, VMEM),
        scratch_shapes=[
            pltpu.VMEM((units, size + width, width), BF16),
            pltpu.VMEM((units, width, width), F32),
            pltpu.VMEM((units, size), F32),
            pltpu.VMEM((units, size), F32),
            pltpu.VMEM((2 * heads, width, 2 * width), F32),
        ],
        compiler_params=pltpu.CompilerParams(vmem_limit_bytes=40 * 1024 * 1024),
        name="chunk_maps",
    )(queries, keys, values, decay, beta)


def join_kernel(heads, own_ref, all_ref, base_ref, lift_ref, gate_ref, gain_ref, mixed_ref):
    places = all_ref.shape[0]
    width = gain_ref.shape[1]
    length = base_ref.shape[0]
    own = own_ref[0]
    states = [jnp.zeros((width, width), F32) for _ in range(2 * heads)]
    for step in range(places - 1):
        for chain in range(2 * heads):
            place = step if chain < heads else places - 1 - step
            state = states[chain]
            applied = mm(all_ref[place, chain, :, width:], state.astype(BF16)) + all_ref[
                place, chain, :, :width
            ].astype(F32)
            use = place < own if chain < heads else place > own
            states[chain] = jnp.where(use, applied, state)
    lows = [state.astype(BF16) for state in states]
    tile = min(length, 256)

    def body(step, carry):
        rows = pl.ds(pl.multiple_of(step * tile, tile), tile)
        for head in range(heads):
            lanes = slice(head * width, (head + 1) * width)
            joined = (
                base_ref[rows, lanes]
                + mm(lift_ref[head, rows, :], lows[head])
                + mm(lift_ref[heads + head, rows, :], lows[heads + head])
            )
            scale = lax.rsqrt(jnp.mean(joined * joined, axis=1, keepdims=True) + NORM_EPSILON)
            gate = gate_ref[rows, lanes].astype(F32)
            silu = gate / (1.0 + jnp.exp(-gate))
            mixed_ref[rows, lanes] = (joined * scale * gain_ref[...] * silu).astype(BF16)
        return carry

    lax.fori_loop(0, length // tile, body, 0)


def join_heads(heads, own, collected, base, lift, gate, gain):
    return pl.pallas_call(
        functools.partial(join_kernel, heads),
        out_shape=jax.ShapeDtypeStruct(base.shape, BF16),
        in_specs=[SMEM] + [VMEM] * 5,
        out_specs=VMEM,
        compiler_params=pltpu.CompilerParams(vmem_limit_bytes=40 * 1024 * 1024),
        name="join_heads",
    )(own, collected, base, lift, gate, gain)


def shards(
    query_vectors,
    key_vectors,
    value_vectors,
    out_gate,
    decay_rate,
    decay_pre,
    decay_shock,
    beta_pre,
    head_gain,
    w_out,
    tokens,
    norm_gain,
    experts_pick,
    pair_logits,
    group_logits,
    expert_gate,
    expert_up,
    expert_down,
):
    length, heads, width = query_vectors.shape
    log_decay = -decay_rate[:, :, None] * jax.nn.softplus(decay_pre) + decay_shock
    beta_rate = jax.nn.sigmoid(beta_pre)
    base, lift, ends = chunk_maps(
        heads,
        query_vectors.reshape(length, heads * width),
        key_vectors.reshape(length, heads * width),
        value_vectors.reshape(length, heads * width),
        log_decay.reshape(-1, width),
        beta_rate.reshape(-1, width),
    )
    collected = lax.all_gather(ends, "sp", axis=0)
    own = lax.axis_index("sp").astype(jnp.int32).reshape(1)
    mixed_heads = join_heads(
        heads, own, collected, base, lift, out_gate.reshape(length, heads * width), head_gain[None, :]
    )
    local_rows = tokens.shape[0]
    part_sum = jnp.dot(mixed_heads, w_out, preferred_element_type=jnp.float32).astype(jnp.bfloat16)
    branch_sum = lax.psum_scatter(
        lax.optimization_barrier(part_sum).astype(jnp.float32).astype(jnp.bfloat16),
        "tp",
        scatter_dimension=0,
        tiled=True,
    ).astype(jnp.float32)
    residual = tokens.astype(jnp.float32) + branch_sum
    normed = (
        residual
        * lax.rsqrt(jnp.mean(residual * residual, axis=-1, keepdims=True) + NORM_EPSILON)
        * norm_gain
    ).astype(jnp.bfloat16)
    group_count = group_logits.shape[1]
    group_exp = jnp.exp(group_logits)
    group_share = group_exp / jnp.sum(group_exp, axis=-1, keepdims=True)
    group_index_of = experts_pick[:, 0] // GROUP_SIZE
    group_weight = jnp.sum(
        jnp.where(jnp.arange(group_count)[None, :] == group_index_of[:, None], group_share, 0.0),
        axis=1,
    )
    pair_exp = jnp.exp(pair_logits)
    route_weight = pair_exp / jnp.sum(pair_exp, axis=-1, keepdims=True) * group_weight[:, None]
    capacity = local_rows // group_count
    expert_count = lax.axis_size("sp")
    marks = (
        experts_pick[:, :, None] == jnp.arange(expert_count, dtype=jnp.int32)[None, None, :]
    ).astype(F32)
    token = jnp.arange(local_rows, dtype=jnp.int32)
    before = (token[:, None] > token[None, :]).astype(F32)
    earlier = jnp.dot(before, jnp.sum(marks, axis=1))
    slot_number = jnp.sum(marks * earlier[:, None, :], axis=2).astype(jnp.int32)
    slot_place = experts_pick * capacity + slot_number
    slot_index = jnp.arange(expert_count * capacity, dtype=jnp.int32)
    hits = slot_place[:, :, None] == slot_index[None, None, :]
    chooser = jnp.any(hits, axis=1).astype(BF16)
    weights = jnp.sum(jnp.where(hits, route_weight[:, :, None], 0.0), axis=1)
    outgoing = mm(chooser, normed, ((0,), (0,))).astype(jnp.bfloat16)
    outgoing = outgoing.reshape(expert_count, capacity, normed.shape[1])
    arrived = lax.all_to_all(outgoing, "sp", split_axis=0, concat_axis=0, tiled=True)
    source_count, slot_count, model_width = arrived.shape
    row_count = source_count * slot_count
    flat_rows = arrived.reshape(row_count, model_width)
    part_rows = lax.all_gather(flat_rows, "tp", axis=0, tiled=True)
    gate_out = jnp.dot(part_rows, expert_gate[0], preferred_element_type=jnp.float32)
    up_out = jnp.dot(part_rows, expert_up[0], preferred_element_type=jnp.float32)
    hidden = (jax.nn.silu(gate_out) * up_out).astype(jnp.bfloat16)
    product = lax.dot_general(
        hidden, expert_down[0], (((1,), (1,)), ((), ())), preferred_element_type=jnp.float32
    ).astype(jnp.bfloat16)
    summed_out = lax.psum_scatter(
        lax.optimization_barrier(product).astype(jnp.float32).astype(jnp.bfloat16),
        "tp",
        scatter_dimension=0,
        tiled=True,
    )
    expert_rows = summed_out.reshape(source_count, slot_count, model_width)
    results = lax.all_to_all(expert_rows, "sp", split_axis=0, concat_axis=0, tiled=True)
    gathered = results.reshape(expert_count * capacity, normed.shape[1])
    mixture = jnp.dot(weights, gathered.astype(F32), precision=EXACT_PRECISION)
    return (residual + mixture).astype(jnp.bfloat16)


def solution(mesh):
    return jax.shard_map(
        shards,
        mesh=mesh,
        in_specs=(
            P("sp", "tp", None),
            P("sp", "tp", None),
            P("sp", "tp", None),
            P("sp", "tp", None),
            P(None, "tp"),
            P(None, "tp", "sp"),
            P(None, "tp", "sp"),
            P(None, "tp", "sp"),
            P(),
            P("tp", None),
            P(("sp", "tp"), None),
            P(),
            P(("sp", "tp"), None),
            P(("sp", "tp"), None),
            P(("sp", "tp"), None),
            P("sp", None, "tp"),
            P("sp", None, "tp"),
            P("sp", None, "tp"),
        ),
        out_specs=P(("sp", "tp"), None),
        check_vma=False,
    )
```

time: 954 us -> 357 us (0.37); the launches traced: 940 us -> 356 us
  other arithmetic: 346 us -> 3.89 us
  matrix products: 225 us -> 30.2 us
  local copies, waits for them, and re-layouts: 69.5 us -> 6.24 us
  blocking collectives: 52.5 us -> 15.8 us
  waiting for transfers between devices: 227 us -> 260 us
  Pallas kernels: 0 us -> 23.3 us
    another operation x10 -> x0, other arithmetic: 317 us -> none  [the longest x5 316 us: block_sweep(): jax.scipy.linalg.solve_triangular(lower_matrix + identity, right_side, lo...]
    dot_general x144 -> x3, matrix products: 191 us -> 3.14 us  [the longest x1 1.56 us: mm(): lax.dot_general(left, right, (contract, ((), ())), preferred_element_type...]
    all_gather x4 -> x0, blocking collectives: 36.5 us -> none  [the longest x1 10.6 us: shards(): lax.all_gather(backward_shift[None].astype(jnp.bfloat16), 'sp', axis=0, t...]
    all_gather x0 -> x1, waiting for transfers between devices: none -> 29.2 us  [shards(): collected = lax.all_gather(ends, 'sp', axis=0)]
    pallas_call x0 -> x2, Pallas kernels: none -> 23.3 us  [the longest x1 21.5 us: chunk_maps(): pl.pallas_call(functools.partial(chunk_kernel, heads), out_shape=(jax.Sha...]
    slice x9 -> x0, local copies, waits for them, and re-layouts: 19.5 us -> none  [the longest x2 10.4 us: shards(): trailing_part[:, :, per_head_width:]]
    mul x6 -> x0, other arithmetic: 11.9 us -> none  [the longest x2 4.81 us: unit_rows(): vectors * lax.rsqrt(jnp.sum(vectors * vectors, axis=-1, keepdims=True) +...]
    exp x32 -> x0, local copies, waits for them, and re-layouts: 11.3 us -> none  [advance(): jnp.exp(total_in)]
  transfers between devices with their start and end apart: 4 -> 5, of which waited for: 4 -> 5; matrix products, arithmetic and copies ran while one was open for 0% -> 0% of each run, Pallas kernels for 0% -> 0%
where the time goes in v1:
time: 357 us; the launch traced here: 356 us
  waiting for transfers between devices  260 us (73%)
  matrix products  30.2 us (8%)
  Pallas kernels  23.3 us (7%)
  blocking collectives  15.8 us (4%)
  between operations  13.3 us (4%)
  local copies, waits for them, and re-layouts  6.24 us (2%)
  starting transfers between devices  3.96 us (1%)
  other arithmetic  3.89 us (1%)
    reduce_scatter x1, waiting for transfers between devices, shards(): lax.psum_scatter(lax.optimization_barrier(product).astype(jnp.float32).as...  88.2 us
    all_gather x1, waiting for transfers between devices, shards(): part_rows = lax.all_gather(flat_rows, 'tp', axis=0, tiled=True)  80.8 us
    reduce_scatter x1, waiting for transfers between devices, shards(): lax.psum_scatter(lax.optimization_barrier(part_sum).astype(jnp.float32).a...  49.7 us
    all_gather x1, waiting for transfers between devices, shards(): collected = lax.all_gather(ends, 'sp', axis=0)  29.2 us
    pallas_call x1, Pallas kernels, chunk_maps(): pl.pallas_call(functools.partial(chunk_kernel, heads), out_shape=(jax.Sha...  21.5 us
    dot_general x1, matrix products, shards(): lax.dot_general(hidden, expert_down[0], (((1,), (1,)), ((), ())), preferr...  16.8 us
    all_to_all x1, blocking collectives, shards(): lax.all_to_all(outgoing, 'sp', split_axis=0, concat_axis=0, tiled=True)  15.8 us
    all_to_all x1, waiting for transfers between devices, shards(): lax.all_to_all(expert_rows, 'sp', split_axis=0, concat_axis=0, tiled=True)  11.7 us
  transfers between devices with their start and end apart: 5, of which 5 were waited for; matrix products, arithmetic and copies ran while one was open for 0% of the time, Pallas kernels for 0%

profile of v1, /device:TPU:0, one launch (start us, length us, event | category | flops | bytes accessed | tf_op | source)
XLA Modules:
  0.0 356.4 jit_solution(138360478889639285)
XLA Ops:
  6.5 1.2 copy.36
  7.8 0.7 neg.15
  8.5 0.8 fusion.13
  9.3 0.7 add_divide_fusion
  10.1 1.4 copy_bitcast_fusion.1
  11.4 21.5 %chunk_maps.1 = (f32[1024,256]{1,0:T(8,128)S(1)}, bf16[4,1024,128]{2,1,0:T(8,128)(2,1)S(1)}, bf16[4,128,256]{2,1,0:T(8,128)(2,1)}) custom-call(bf16[1024,256]{1,0:T(8,128)(2,1)S(1)} %bitcast.41, bf16[1024,256]{1,0:T(8,128)(2,1)S(1)} %get-tuple-element.14.k_ref, bf16[1024,256]{1,0:T(8,128)(2,1)S(1)} %get-tuple-element.13.v_ref, ...), custom_call_target="tpu_custom_call" | custom-call | tf_op jit(solution)/shard_map/chunk_maps/pallas_call | solution.py:144
  32.9 1.0 copy-done.1
  34.1 29.2 %all-gather.6.cloned.1.call-done = bf16[16,128,256]{2,1,0:T(8,128)(2,1)} async-done(((bf16[4,128,256]{2,1,0:T(8,128)(2,1)}), bf16[16,128,256]{2,1,0:T(8,128)(2,1)}) %all-gather.6.cloned.1.call-update) | async-done | bytes 1048592 | tf_op jit(solution)/shard_map/all_gather | solution.py:243
  63.3 1.2 copy-done.2
  64.6 1.2 copy-done.3
  65.8 1.9 join_heads.1
  67.7 3.2 convolution_convert_fusion.1
  71.3 49.7 %reduce-scatter.3.cloned.1.call-done = bf16[128,2048]{1,0:T(8,128)(2,1)} async-done(((bf16[1024,2048]{1,0:T(8,128)(2,1)}), bf16[128,2048]{1,0:T(8,128)(2,1)}) %reduce-scatter.3.cloned.1.call-update) | async-done | bytes 524304 | tf_op jit(solution)/shard_map/reduce_scatter | solution.py:250
  121.0 1.3 multiply_reduce_fusion
  122.3 1.6 convolution_convert_fusion.2
  123.9 15.8 %all_to_all.10 = bf16[4,64,2048]{2,1,0:T(8,128)(2,1)} all-to-all(bf16[4,64,2048]{2,1,0:T(8,128)(2,1)S(1)} %bitcast.45), channel_id=1, replica_groups=mesh['sp'=4,'tp'=8] {'sp'}, dimensions={0} | all-to-all | bytes 2097152 | tf_op jit(solution)/shard_map/all_to_all | solution.py:288
  139.7 0.2 reduce-scatter.5.cloned.1.call-start
  140.0 80.8 %all-gather.4.cloned.1.call-done = bf16[2048,2048]{1,0:T(8,128)(2,1)} async-done(((bf16[256,2048]{1,0:T(8,128)(2,1)}), bf16[2048,2048]{1,0:T(8,128)(2,1)}) %all-gather.4.cloned.1.call-update) | async-done | bytes 8388624 | tf_op jit(solution)/shard_map/all_gather | solution.py:292
  220.8 7.1 %fusion.5 = f32[2048,256]{1,0:T(8,128)} fusion(bf16[2048,2048]{1,0:T(8,128)(2,1)} %all-gather.4.cloned.1.call-done, bf16[1,2048,256]{2,1,0:T(8,128)(2,1)S(1)} %copy-done.13), kind=kOutput, calls=%fused_computation.9 | convolution fusion | flops 2147483648 | bytes 11534336 | tf_op jit(solution)/shard_map/dot_general | solution.py:293
  227.9 16.8 %convolution_convert_fusion = bf16[2048,2048]{1,0:T(8,128)(2,1)} fusion(bf16[2048,2048]{1,0:T(8,128)(2,1)} %all-gather.4.cloned.1.call-done, f32[2048,256]{1,0:T(8,128)} %fusion.5, bf16[1,2048,256]{2,1,0:T(8,128)(2,1)S(1)} %copy-done, bf16[1,2048,256]{2,1,0:T(8,128)(2,1)} %param.34), kind=kOutput, calls=%fused_computation | convolution fusion | flops 4302307328 | bytes 20971520 | tf_op jit(solution)/shard_map/dot_general | solution.py:296
  244.7 88.2 %reduce-scatter.5.cloned.1.call-done = bf16[256,2048]{1,0:T(8,128)(2,1)} async-done(((bf16[2048,2048]{1,0:T(8,128)(2,1)}), bf16[256,2048]{1,0:T(8,128)(2,1)}) %reduce-scatter.5.cloned.1.call-update) | async-done | bytes 1048592 | tf_op jit(solution)/shard_map/reduce_scatter | solution.py:299
  332.9 3.6 %all-to-all-start.1 = ((bf16[4,64,2048]{2,1,0:T(8,128)(2,1)}), bf16[4,64,2048]{2,1,0:T(8,128)(2,1)S(1)}, u32[]{:S(2)}, u32[]{:S(2)}) async-start(bf16[4,64,2048]{2,1,0:T(8,128)(2,1)} %bitcast.48), calls=%async_computation.3 | async-start | bytes 2097152 | tf_op jit(solution)/shard_map/all_to_all | solution.py:306
  336.7 11.7 %all-to-all-done.1 = bf16[4,64,2048]{2,1,0:T(8,128)(2,1)S(1)} async-done(((bf16[4,64,2048]{2,1,0:T(8,128)(2,1)}), bf16[4,64,2048]{2,1,0:T(8,128)(2,1)S(1)}, u32[]{:S(2)}, u32[]{:S(2)}) %all-to-all-start.1) | async-done | bytes 1048608 | tf_op jit(solution)/shard_map/all_to_all | solution.py:306
  348.4 1.4 fusion.1
  (46 shorter events, 0.8 us)
Async XLA Ops:
  6.5 221.3 %copy-start = (bf16[1,2048,256]{2,1,0:T(8,128)(2,1)S(1)}, bf16[1,2048,256]{2,1,0:T(8,128)(2,1)}, u32[]{:S(2)}) copy-start(bf16[1,2048,256]{2,1,0:T(8,128)(2,1)} %param.35) | copy-start | bytes 3145732
  6.5 27.5 %copy-start.8 = (bf16[1024,2,128]{2,1,0:T(2,128)(2,1)S(1)}, bf16[1024,2,128]{2,1,0:T(2,128)(2,1)}, u32[]{:S(2)}) copy-start(bf16[1024,2,128]{2,1,0:T(2,128)(2,1)} %param.21) | copy-start | bytes 1572868
  6.5 56.8 %copy-start.4 = (f32[128]{0:T(128)S(1)}, f32[128]{0:T(128)}, u32[]{:S(2)}) copy-start(f32[128]{0:T(128)} %param.26) | copy-start | bytes 1540
  6.5 56.8 %all-gather.6.cloned.1.call-start = ((), (), s32[]{:S(2)}) async-start(), calls=%async_computation.7 | async-start | bytes 1310720 | tf_op jit(solution)/shard_map/all_gather | solution.py:243
  32.9 1.0 copy-start.1
  33.9 87.1 %reduce-scatter.3.cloned.1.call-start = ((), (), s32[]{:S(2)}) async-start(), calls=%async_computation.4 | async-start | bytes 4718592 | tf_op jit(solution)/shard_map/reduce_scatter | solution.py:250
  63.3 1.2 copy-start.2
  64.6 1.2 copy-start.3
  65.8 1.9 copy-start.7
  67.7 3.3 copy-start.9
  67.7 53.3 %copy-start.5 = (bf16[128,2048]{1,0:T(8,128)(2,1)S(1)}, bf16[128,2048]{1,0:T(8,128)(2,1)}, u32[]{:S(2)}) copy-start(bf16[128,2048]{1,0:T(8,128)(2,1)} %param.28) | copy-start | bytes 1572868
  70.9 51.4 %copy-start.10 = (f32[2048]{0:T(1024)S(1)}, f32[2048]{0:T(1024)}, u32[]{:S(2)}) copy-start(f32[2048]{0:T(1024)} %param.29) | copy-start | bytes 24580
  70.9 149.9 %copy-start.13 = (bf16[1,2048,256]{2,1,0:T(8,128)(2,1)S(1)}, bf16[1,2048,256]{2,1,0:T(8,128)(2,1)}, u32[]{:S(2)}) copy-start(bf16[1,2048,256]{2,1,0:T(8,128)(2,1)} %param.33) | copy-start | bytes 3145732
  70.9 149.8 %all-gather.4.cloned.1.call-start = ((), (), s32[]{:S(2)}) async-start(), calls=%async_computation.5 | async-start | bytes 9437184 | tf_op jit(solution)/shard_map/all_gather | solution.py:292
  139.7 193.1 %reduce-scatter.5.cloned.1.call-start = ((), (), s32[]{:S(2)}) async-start(), calls=%async_computation.6 | async-start | bytes 9437184 | tf_op jit(solution)/shard_map/reduce_scatter | solution.py:299
  244.7 91.9 %copy-start.12 = (f32[128,2]{0,1:T(2,128)S(1)}, f32[128,2]{0,1:T(2,128)}, u32[]{:S(2)}) copy-start(f32[128,2]{0,1:T(2,128)} %param.32) | copy-start | bytes 3076
  244.7 91.9 %copy-start.11 = (f32[128,2]{0,1:T(2,128)S(1)}, f32[128,2]{0,1:T(2,128)}, u32[]{:S(2)}) copy-start(f32[128,2]{0,1:T(2,128)} %param.31) | copy-start | bytes 3076
  244.7 103.7 %copy-start.6 = (bf16[128,2048]{1,0:T(8,128)(2,1)S(1)}, bf16[128,2048]{1,0:T(8,128)(2,1)}, u32[]{:S(2)}) copy-start(bf16[128,2048]{1,0:T(8,128)(2,1)} %reduce-scatter.3.cloned.1.call-done) | copy-start | bytes 1572868
  332.9 15.5 %all-to-all-start.1 = ((bf16[4,64,2048]{2,1,0:T(8,128)(2,1)}), bf16[4,64,2048]{2,1,0:T(8,128)(2,1)S(1)}, u32[]{:S(2)}, u32[]{:S(2)}) async-start(bf16[4,64,2048]{2,1,0:T(8,128)(2,1)} %bitcast.48), calls=%async_computation.3 | async-start | bytes 2097152 | tf_op jit(solution)/shard_map/all_to_all | solution.py:306
Sparse Core Ops, SparseCore 0:
  34.1 29.2 all-gather.5
  71.0 49.9 reduce-scatter.2
  139.8 80.8 all-gather.3
  244.8 88.0 reduce-scatter.4

commit v2 on v1

--- a/solution.py
+++ b/solution.py
@@ -5,6 +5,7 @@
 from jax import lax
 from jax.experimental import pallas as pl
 from jax.experimental.pallas import tpu as pltpu
+from jax.sharding import Mesh
 from jax.sharding import PartitionSpec as P
 
 GROUP_SIZE = 2
@@ -240,8 +241,8 @@
         log_decay.reshape(-1, width),
         beta_rate.reshape(-1, width),
     )
-    collected = lax.all_gather(ends, "sp", axis=0)
-    own = lax.axis_index("sp").astype(jnp.int32).reshape(1)
+    collected = lax.all_gather(ends, ("grp", "mate"), axis=0)
+    own = lax.axis_index(("grp", "mate")).astype(jnp.int32).reshape(1)
     mixed_heads = join_heads(
         heads, own, collected, base, lift, out_gate.reshape(length, heads * width), head_gain[None, :]
     )
@@ -259,80 +260,86 @@
         * lax.rsqrt(jnp.mean(residual * residual, axis=-1, keepdims=True) + NORM_EPSILON)
         * norm_gain
     ).astype(jnp.bfloat16)
-    group_count = group_logits.shape[1]
+    mates = lax.axis_size("mate")
+    group_count = lax.axis_size("grp")
+    group_of = experts_pick[:, 0] // GROUP_SIZE
+    capacity = local_rows // group_count
+    member = (group_of[:, None] == jnp.arange(group_count, dtype=jnp.int32)[None, :]).astype(F32)
+    token = jnp.arange(local_rows, dtype=jnp.int32)
+    before = (token[:, None] > token[None, :]).astype(F32)
+    rank = jnp.sum(member * jnp.dot(before, member), axis=1).astype(jnp.int32)
+    place = group_of * capacity + rank
+    chooser = place[:, None] == token[None, :]
     group_exp = jnp.exp(group_logits)
     group_share = group_exp / jnp.sum(group_exp, axis=-1, keepdims=True)
-    group_index_of = experts_pick[:, 0] // GROUP_SIZE
-    group_weight = jnp.sum(
-        jnp.where(jnp.arange(group_count)[None, :] == group_index_of[:, None], group_share, 0.0),
-        axis=1,
-    )
+    group_weight = jnp.sum(member * group_share, axis=1)
     pair_exp = jnp.exp(pair_logits)
     route_weight = pair_exp / jnp.sum(pair_exp, axis=-1, keepdims=True) * group_weight[:, None]
-    capacity = local_rows // group_count
-    expert_count = lax.axis_size("sp")
-    marks = (
-        experts_pick[:, :, None] == jnp.arange(expert_count, dtype=jnp.int32)[None, None, :]
-    ).astype(F32)
-    token = jnp.arange(local_rows, dtype=jnp.int32)
-    before = (token[:, None] > token[None, :]).astype(F32)
-    earlier = jnp.dot(before, jnp.sum(marks, axis=1))
-    slot_number = jnp.sum(marks * earlier[:, None, :], axis=2).astype(jnp.int32)
-    slot_place = experts_pick * capacity + slot_number
-    slot_index = jnp.arange(expert_count * capacity, dtype=jnp.int32)
-    hits = slot_place[:, :, None] == slot_index[None, None, :]
-    chooser = jnp.any(hits, axis=1).astype(BF16)
-    weights = jnp.sum(jnp.where(hits, route_weight[:, :, None], 0.0), axis=1)
-    outgoing = mm(chooser, normed, ((0,), (0,))).astype(jnp.bfloat16)
-    outgoing = outgoing.reshape(expert_count, capacity, normed.shape[1])
-    arrived = lax.all_to_all(outgoing, "sp", split_axis=0, concat_axis=0, tiled=True)
-    source_count, slot_count, model_width = arrived.shape
-    row_count = source_count * slot_count
-    flat_rows = arrived.reshape(row_count, model_width)
-    part_rows = lax.all_gather(flat_rows, "tp", axis=0, tiled=True)
-    gate_out = jnp.dot(part_rows, expert_gate[0], preferred_element_type=jnp.float32)
-    up_out = jnp.dot(part_rows, expert_up[0], preferred_element_type=jnp.float32)
-    hidden = (jax.nn.silu(gate_out) * up_out).astype(jnp.bfloat16)
-    product = lax.dot_general(
-        hidden, expert_down[0], (((1,), (1,)), ((), ())), preferred_element_type=jnp.float32
-    ).astype(jnp.bfloat16)
-    summed_out = lax.psum_scatter(
-        lax.optimization_barrier(product).astype(jnp.float32).astype(jnp.bfloat16),
-        "tp",
-        scatter_dimension=0,
-        tiled=True,
-    )
-    expert_rows = summed_out.reshape(source_count, slot_count, model_width)
-    results = lax.all_to_all(expert_rows, "sp", split_axis=0, concat_axis=0, tiled=True)
-    gathered = results.reshape(expert_count * capacity, normed.shape[1])
-    mixture = jnp.dot(weights, gathered.astype(F32), precision=EXACT_PRECISION)
-    return (residual + mixture).astype(jnp.bfloat16)
+    mate_weight = [
+        jnp.sum(jnp.where(experts_pick % GROUP_SIZE == mate, route_weight, 0.0), axis=1)
+        for mate in range(GROUP_SIZE)
+    ]
+    lane = jnp.arange(width, dtype=jnp.int32)[None, None, :]
+    spread = sum(
+        jnp.where(lane == mate, mate_weight[mate][:, None, None], 0.0) for mate in range(GROUP_SIZE)
+    )
+    slot_weight = jnp.sum(jnp.where(chooser[:, :, None], spread, 0.0), axis=0)
+    all_weight = lax.all_gather(slot_weight, ("grp", "mate", "tp"), axis=0)
+    tp_count = lax.axis_size("tp")
+    all_weight = all_weight[:, :, :GROUP_SIZE].reshape(
+        group_count, mates, tp_count, group_count, capacity, GROUP_SIZE
+    )
+    own_grp = lax.axis_index("grp")
+    own_mate = lax.axis_index("mate")
+    own_weight = lax.dynamic_index_in_dim(all_weight, own_grp, 3, keepdims=False)
+    own_weight = lax.dynamic_index_in_dim(own_weight, own_mate, 4, keepdims=False)
+    own_weight = jnp.transpose(own_weight, (1, 2, 0, 3)).reshape(-1, 1)
+    outgoing = mm(chooser.astype(BF16), normed, ((0,), (0,))).astype(BF16)
+    outgoing = outgoing.reshape(group_count, capacity, normed.shape[1])
+    arrived = lax.all_to_all(outgoing, "grp", split_axis=0, concat_axis=0, tiled=True)
+    flat_rows = arrived.reshape(local_rows, normed.shape[1])
+    part_rows = lax.all_gather(flat_rows, ("mate", "tp"), axis=0, tiled=True)
+    gate_out = jnp.dot(part_rows, expert_gate[0], preferred_element_type=F32)
+    up_out = jnp.dot(part_rows, expert_up[0], preferred_element_type=F32)
+    hidden = (jax.nn.silu(gate_out) * up_out * own_weight).astype(BF16)
+    product = mm(hidden, expert_down[0], ((1,), (1,))).astype(BF16)
+    summed_out = lax.psum_scatter(product, ("mate", "tp"), scatter_dimension=0, tiled=True)
+    expert_rows = summed_out.reshape(group_count, capacity, normed.shape[1])
+    results = lax.all_to_all(expert_rows, "grp", split_axis=0, concat_axis=0, tiled=True)
+    gathered = results.reshape(local_rows, normed.shape[1])
+    mixture = mm(chooser.astype(BF16), gathered)
+    return (residual + mixture).astype(BF16)
 
 
 def solution(mesh):
+    places, inner = mesh.devices.shape
+    mesh = Mesh(
+        mesh.devices.reshape(places // GROUP_SIZE, GROUP_SIZE, inner), ("grp", "mate", "tp")
+    )
+    sp = ("grp", "mate")
     return jax.shard_map(
         shards,
         mesh=mesh,
         in_specs=(
-            P("sp", "tp", None),
-            P("sp", "tp", None),
-            P("sp", "tp", None),
-            P("sp", "tp", None),
+            P(sp, "tp", None),
+            P(sp, "tp", None),
+            P(sp, "tp", None),
+            P(sp, "tp", None),
             P(None, "tp"),
-            P(None, "tp", "sp"),
-            P(None, "tp", "sp"),
-            P(None, "tp", "sp"),
+            P(None, "tp", sp),
+            P(None, "tp", sp),
+            P(None, "tp", sp),
             P(),
             P("tp", None),
-            P(("sp", "tp"), None),
+            P(("grp", "mate", "tp"), None),
             P(),
-            P(("sp", "tp"), None),
-            P(("sp", "tp"), None),
-            P(("sp", "tp"), None),
-            P("sp", None, "tp"),
-            P("sp", None, "tp"),
-            P("sp", None, "tp"),
+            P(("grp", "mate", "tp"), None),
+            P(("grp", "mate", "tp"), None),
+            P(("grp", "mate", "tp"), None),
+            P(sp, None, "tp"),
+            P(sp, None, "tp"),
+            P(sp, None, "tp"),
         ),
-        out_specs=P(("sp", "tp"), None),
+        out_specs=P(("grp", "mate", "tp"), None),
         check_vma=False,
     )

time: 357 us -> 367 us (1.028)
  blocking collectives: 15.8 us -> 24.2 us
  matrix products: 30.2 us -> 26.4 us
  starting transfers between devices: 3.96 us -> 0.18 us
    dot_general x4 -> x2, matrix products: 25.5 us -> 7.45 us  [the longest x1 7.3 us: shards(): gate_out = jnp.dot(part_rows, expert_gate[0], preferred_element_type=F32)]
    dot_general x1 -> x3, matrix products: 1.56 us -> 15.8 us  [mm(): lax.dot_general(left, right, (contract, ((), ())), preferred_element_type...]
    reduce_scatter x1, waiting for transfers between devices: 88.2 us -> 102 us  [shards(): lax.psum_scatter(product, ('mate', 'tp'), scatter_dimension=0, tiled=True)]
    all_to_all x1 -> x0, waiting for transfers between devices: 11.7 us -> none  [shards(): lax.all_to_all(expert_rows, 'sp', split_axis=0, concat_axis=0, tiled=True)]
    all_to_all x1 -> x2, blocking collectives: 15.8 us -> 24.2 us  [the longest x1 13 us: shards(): lax.all_to_all(outgoing, 'grp', split_axis=0, concat_axis=0, tiled=True)]
    all_gather x2 -> x3, waiting for transfers between devices: 110 us -> 109 us  [the longest x1 73.3 us: shards(): part_rows = lax.all_gather(flat_rows, ('mate', 'tp'), axis=0, tiled=True)]
  transfers between devices with their start and end apart: 5 -> 5, of which waited for: 5 -> 5; matrix products, arithmetic and copies ran while one was open for 0% -> 3% of each run, Pallas kernels for 0% -> 0%
where the time goes in v2:
time: 367 us; the launch traced here: 366 us
  waiting for transfers between devices  260 us (71%)
  matrix products  26.4 us (7%)
  blocking collectives  24.2 us (7%)
  Pallas kernels  23.3 us (6%)
  between operations  15.2 us (4%)
  local copies, waits for them, and re-layouts  9.2 us (3%)
  other arithmetic  7.35 us (2%)
    reduce_scatter x1, waiting for transfers between devices, shards(): lax.psum_scatter(product, ('mate', 'tp'), scatter_dimension=0, tiled=True)  102 us
    all_gather x1, waiting for transfers between devices, shards(): part_rows = lax.all_gather(flat_rows, ('mate', 'tp'), axis=0, tiled=True)  73.3 us
    reduce_scatter x1, waiting for transfers between devices, shards(): lax.psum_scatter(lax.optimization_barrier(part_sum).astype(jnp.float32).a...  49.3 us
    all_gather x1, waiting for transfers between devices, shards(): collected = lax.all_gather(ends, ('grp', 'mate'), axis=0)  28.2 us
    pallas_call x1, Pallas kernels, chunk_maps(): pl.pallas_call(functools.partial(chunk_kernel, heads), out_shape=(jax.Sha...  21.5 us
    dot_general x3, matrix products, mm(): lax.dot_general(left, right, (contract, ((), ())), preferred_element_type...  15.8 us
    all_to_all x1, blocking collectives, shards(): lax.all_to_all(outgoing, 'grp', split_axis=0, concat_axis=0, tiled=True)  13 us
    all_to_all x1, blocking collectives, shards(): lax.all_to_all(expert_rows, 'grp', split_axis=0, concat_axis=0, tiled=True)  11.1 us
  transfers between devices with their start and end apart: 5, of which 5 were waited for; matrix products, arithmetic and copies ran while one was open for 3% of the time, Pallas kernels for 0%

profile of v2, /device:TPU:0, one launch (start us, length us, event | category | flops | bytes accessed | tf_op | source)
XLA Modules:
  0.0 366.2 jit_solution(7415390867799904727)
XLA Ops:
  8.2 0.8 fusion.16
  9.8 1.1 copy.36
  10.9 1.4 copy_bitcast_fusion.1
  12.3 21.5 %chunk_maps.1 = (f32[1024,256]{1,0:T(8,128)S(1)}, bf16[4,1024,128]{2,1,0:T(8,128)(2,1)S(1)}, bf16[4,128,256]{2,1,0:T(8,128)(2,1)}) custom-call(bf16[1024,256]{1,0:T(8,128)(2,1)S(1)} %bitcast.51, bf16[1024,256]{1,0:T(8,128)(2,1)S(1)} %get-tuple-element.14.k_ref, bf16[1024,256]{1,0:T(8,128)(2,1)S(1)} %get-tuple-element.13.v_ref, ...), custom_call_target="tpu_custom_call" | custom-call | tf_op jit(solution)/shard_map/chunk_maps/pallas_call | solution.py:145
  33.7 1.0 copy-done.1
  34.8 1.1 copy.35
  35.9 28.2 %all-gather.8.cloned.1.call-done = bf16[16,128,256]{2,1,0:T(8,128)(2,1)} async-done(((bf16[4,128,256]{2,1,0:T(8,128)(2,1)}), bf16[16,128,256]{2,1,0:T(8,128)(2,1)}) %all-gather.8.cloned.1.call-update) | async-done | bytes 1048592 | tf_op jit(solution)/shard_map/all_gather | solution.py:244
  64.1 1.2 copy-done.2
  65.4 1.2 copy-done.3
  66.6 1.8 join_heads.1
  68.5 3.2 convolution_convert_fusion.1
  72.3 3.4 select_reduce_fusion
  75.8 49.3 %reduce-scatter.3.cloned.1.call-done = bf16[128,2048]{1,0:T(8,128)(2,1)} async-done(((bf16[1024,2048]{1,0:T(8,128)(2,1)}), bf16[128,2048]{1,0:T(8,128)(2,1)}) %reduce-scatter.3.cloned.1.call-update) | async-done | bytes 524304 | tf_op jit(solution)/shard_map/reduce_scatter | solution.py:251
  125.0 1.3 multiply_reduce_fusion
  126.3 1.5 convolution_convert_fusion.2
  127.8 13.0 %all_to_all.10 = bf16[2,64,2048]{2,1,0:T(8,128)(2,1)} all-to-all(bf16[2,64,2048]{2,1,0:T(8,128)(2,1)S(1)} %bitcast.56), channel_id=1, replica_groups=mesh['grp'=2,'mate'=2,'tp'=8] {'grp'}, dimensions={0} | all-to-all | bytes 1048576 | tf_op jit(solution)/shard_map/all_to_all | solution.py:299
  140.9 7.3 %all-gather.10.cloned.1.call-done = f32[4096,128]{1,0:T(8,128)} async-done(((f32[128,128]{1,0:T(8,128)}), f32[4096,128]{1,0:T(8,128)}) %all-gather.10.cloned.1.call-update) | async-done | bytes 2097168 | tf_op jit(solution)/shard_map/all_gather | solution.py:287
  148.3 1.6 constant_dynamic-slice_fusion
  150.3 73.3 %all-gather.6.cloned.1.call-done = bf16[2048,2048]{1,0:T(8,128)(2,1)} async-done(((bf16[128,2048]{1,0:T(8,128)(2,1)}), bf16[2048,2048]{1,0:T(8,128)(2,1)}) %all-gather.6.cloned.1.call-update) | async-done | bytes 8388624 | tf_op jit(solution)/shard_map/all_gather | solution.py:301
  223.6 7.3 %fusion.7 = f32[2048,256]{1,0:T(8,128)} fusion(bf16[2048,2048]{1,0:T(8,128)(2,1)} %all-gather.6.cloned.1.call-done, bf16[1,2048,256]{2,1,0:T(8,128)(2,1)} %param.33), kind=kOutput, calls=%fused_computation.13 | convolution fusion | flops 2147483648 | bytes 11534336 | tf_op jit(solution)/shard_map/dot_general | solution.py:302
  230.9 13.1 %convolution_convert_fusion = bf16[2048,2048]{1,0:T(8,128)(2,1)} fusion(bf16[2048,2048]{1,0:T(8,128)(2,1)} %all-gather.6.cloned.1.call-done, f32[2048,256]{1,0:T(8,128)} %fusion.7, bf16[1,2048,256]{2,1,0:T(8,128)(2,1)S(1)} %copy-done, bf16[1,2048,256]{2,1,0:T(8,128)(2,1)S(1)} %copy-done.12, f32[2048]{0:T(1024)S(1)} %mul.84), kind=kOutput, calls=%fused_computation.1 | convolution fusion | flops 4302831616 | bytes 20979712 | tf_op jit(solution)/shard_map/dot_general | solution.py:22
  244.1 102.2 %reduce-scatter.5.cloned.1.call-done = bf16[128,2048]{1,0:T(8,128)(2,1)} async-done(((bf16[2048,2048]{1,0:T(8,128)(2,1)}), bf16[128,2048]{1,0:T(8,128)(2,1)}) %reduce-scatter.5.cloned.1.call-update) | async-done | bytes 524304 | tf_op jit(solution)/shard_map/reduce_scatter | solution.py:306
  346.3 11.1 %all_to_all.11 = bf16[2,64,2048]{2,1,0:T(8,128)(2,1)S(1)} all-to-all(bf16[2,64,2048]{2,1,0:T(8,128)(2,1)} %bitcast.59), channel_id=1, replica_groups=mesh['grp'=2,'mate'=2,'tp'=8] {'grp'}, dimensions={0} | all-to-all | bytes 1048576 | tf_op jit(solution)/shard_map/all_to_all | solution.py:308
  357.4 1.2 fusion.2
  (51 shorter events, 2.8 us)
Async XLA Ops:
  7.4 223.6 %copy-start = (bf16[1,2048,256]{2,1,0:T(8,128)(2,1)S(1)}, bf16[1,2048,256]{2,1,0:T(8,128)(2,1)}, u32[]{:S(2)}) copy-start(bf16[1,2048,256]{2,1,0:T(8,128)(2,1)} %param.35) | copy-start | bytes 3145732
  7.4 56.8 %copy-start.4 = (f32[128]{0:T(128)S(1)}, f32[128]{0:T(128)}, u32[]{:S(2)}) copy-start(f32[128]{0:T(128)} %param.26) | copy-start | bytes 1540
  7.4 56.8 %all-gather.8.cloned.1.call-start = ((), (), s32[]{:S(2)}) async-start(), calls=%async_computation.7 | async-start | bytes 1310720 | tf_op jit(solution)/shard_map/all_gather | solution.py:244
  33.7 1.0 copy-start.1
  34.7 90.3 %reduce-scatter.3.cloned.1.call-start = ((), (), s32[]{:S(2)}) async-start(), calls=%async_computation.4 | async-start | bytes 4718592 | tf_op jit(solution)/shard_map/reduce_scatter | solution.py:251
  64.1 1.2 copy-start.2
  65.4 1.2 copy-start.3
  66.6 1.9 copy-start.7
  68.4 3.3 copy-start.10
  68.5 3.3 copy-start.9
  68.5 3.4 copy-start.11
  71.7 53.3 %copy-start.5 = (bf16[128,2048]{1,0:T(8,128)(2,1)S(1)}, bf16[128,2048]{1,0:T(8,128)(2,1)}, u32[]{:S(2)}) copy-start(bf16[128,2048]{1,0:T(8,128)(2,1)} %param.28) | copy-start | bytes 1572868
  71.7 54.6 %copy-start.8 = (f32[2048]{0:T(1024)S(1)}, f32[2048]{0:T(1024)}, u32[]{:S(2)}) copy-start(f32[2048]{0:T(1024)} %param.29) | copy-start | bytes 24580
  71.7 76.5 %all-gather.10.cloned.1.call-start = ((), (), s32[]{:S(2)}) async-start(), calls=%async_computation.8 | async-start | bytes 2162688 | tf_op jit(solution)/shard_map/all_gather | solution.py:287
  75.7 147.9 %all-gather.6.cloned.1.call-start = ((), (), s32[]{:S(2)}) async-start(), calls=%async_computation.5 | async-start | bytes 8912896 | tf_op jit(solution)/shard_map/all_gather | solution.py:301
  140.8 205.5 %reduce-scatter.5.cloned.1.call-start = ((), (), s32[]{:S(2)}) async-start(), calls=%async_computation.6 | async-start | bytes 8912896 | tf_op jit(solution)/shard_map/reduce_scatter | solution.py:306
  150.3 80.6 %copy-start.12 = (bf16[1,2048,256]{2,1,0:T(8,128)(2,1)S(1)}, bf16[1,2048,256]{2,1,0:T(8,128)(2,1)}, u32[]{:S(2)}) copy-start(bf16[1,2048,256]{2,1,0:T(8,128)(2,1)} %param.34) | copy-start | bytes 3145732
  244.1 113.4 %copy-start.6 = (bf16[128,2048]{1,0:T(8,128)(2,1)S(1)}, bf16[128,2048]{1,0:T(8,128)(2,1)}, u32[]{:S(2)}) copy-start(bf16[128,2048]{1,0:T(8,128)(2,1)} %reduce-scatter.3.cloned.1.call-done) | copy-start | bytes 1572868
Sparse Core Ops, SparseCore 0:
  34.9 29.2 all-gather.7
  71.8 53.1 reduce-scatter.2
Sparse Core Ops, SparseCore 1:
  75.8 72.4 all-gather.9
  150.3 73.2 all-gather.5
  244.2 102.1 reduce-scatter.4
